TPU v7x, 32 devices: a whole 2x2x4 slice. The times are simulated.
32 devices in a mesh: fs: 8 (over z, x), tp: 4 (over y, core).
Axes of the slice: x: 2, y: 2, z: 4, core: 2. Of those that a mesh axis runs over, the one named last changes fastest.
Arguments:
- tokens: bfloat16 [4096, 2048], P(('fs', 'tp')), may hold values from -6 to 6
- gate_weight: bfloat16 [2048, 6144], P('fs', 'tp'), may hold values from -0.125 to 0.125
- value_weight: bfloat16 [2048, 6144], P('fs', 'tp'), may hold values from -0.125 to 0.125
- gate_taps: float32 [3, 6144], P(None, 'tp'), may hold values from -3.5 to 3.5
- value_taps: float32 [3, 6144], P(None, 'tp'), may hold values from -3.5 to 3.5
- down_weight: bfloat16 [6144, 2048], P('tp', 'fs'), may hold values from -0.078125 to 0.078125
- norm_gain: float32 [2048], replicated, may hold values from 0.1 to 1.9
- norm_shift: float32 [2048], replicated, may hold values from -3 to 3
Outputs:
- mixed: bfloat16 [4096, 2048], P(('fs', 'tp'))
All inputs are finite; a program needn't handle non-finite values.
Results may differ from a plain program's by a relative error of at most 0.017.
Values may be sent and summed in bfloat16 or wider, within the bound.
A program may use at most 256 MiB of HBM per device.

v0:
```python
import jax
import jax.numpy as jnp
from jax import lax
from jax.sharding import PartitionSpec as P


def causal_mix(pre, kernel_taps):
    leading = jnp.zeros((2, pre.shape[1]), jnp.float32)
    padded = jnp.concatenate([leading, pre.astype(jnp.float32)], axis=0)
    length = pre.shape[0]
    return (
        kernel_taps[0] * padded[0:length]
        + kernel_taps[1] * padded[1 : length + 1]
        + kernel_taps[2] * padded[2 : length + 2]
    )


def local(
    tokens, gate_weight, value_weight, gate_taps, value_taps, down_weight, norm_gain, norm_shift
):
    sequence = lax.all_gather(tokens, "tp", axis=0, tiled=True)

    def add_rows(segment):
        return jnp.dot(sequence, segment, preferred_element_type=jnp.float32)

    gate_sum = add_rows(lax.all_gather(gate_weight, "fs", axis=0, tiled=True))
    value_sum = add_rows(lax.all_gather(value_weight, "fs", axis=0, tiled=True))
    gate_mix = causal_mix(gate_sum.astype(jnp.bfloat16), gate_taps)
    value_mix = causal_mix(value_sum.astype(jnp.bfloat16), value_taps)
    hidden = (jax.nn.gelu(gate_mix, approximate=False) * value_mix).astype(jnp.bfloat16)
    partial_terms = jnp.dot(
        hidden,
        lax.all_gather(down_weight, "fs", axis=1, tiled=True),
        preferred_element_type=jnp.float32,
    )
    summed = lax.psum_scatter(
        partial_terms.astype(jnp.bfloat16), "tp", scatter_dimension=0, tiled=True
    ).astype(jnp.float32)
    average = jnp.mean(summed, axis=1, keepdims=True)
    centered = summed - average
    variance = jnp.mean(centered * centered, axis=1, keepdims=True)
    normed = centered * lax.rsqrt(variance + 1e-05) * norm_gain + norm_shift
    return normed.astype(jnp.bfloat16)


def solution(mesh):
    in_specs = (
        P(("fs", "tp"), None),
        P("fs", "tp"),
        P("fs", "tp"),
        P(None, "tp"),
        P(None, "tp"),
        P("tp", "fs"),
        P(),
        P(),
    )
    out_specs = P(("fs", "tp"), None)
    return jax.shard_map(local, mesh=mesh, in_specs=in_specs, out_specs=out_specs, check_vma=False)
```

profile of v0, /device:TPU:0, one launch (start us, length us, event | category | flops | bytes accessed | tf_op | source)
XLA Modules:
  0.0 394.9 jit_solution(5087503630397722218)
XLA Ops:
  6.5 0.0 all-gather.5.cloned.1.call-start
  6.5 0.7 all-gather.5.cloned.1.call-update
  7.3 0.0 all-gather.7.cloned.1.call-start
  7.3 0.7 all-gather.7.cloned.1.call-update
  8.0 0.0 all-gather.9.cloned.1.call-start
  8.1 0.7 all-gather.9.cloned.1.call-update
  8.7 0.0 all-gather.11.cloned.1.call-start
  8.8 0.5 all-gather.11.cloned.1.call-update
  9.3 0.0 reduce-scatter.2.cloned.1.call-start
  9.4 1.0 slice_reduce_fusion.2
  10.3 23.9 %all-gather.5.cloned.1.call-done = bf16[512,2048]{1,0:T(8,128)(2,1)} async-done(((bf16[128,2048]{1,0:T(8,128)(2,1)}), bf16[512,2048]{1,0:T(8,128)(2,1)}) %all-gather.5.cloned.1.call-update) | async-done | bytes 2097168 | tf_op jit(solution)/shard_map/all_gather | solution.py:21
  34.2 0.0 copy-start.2
  34.2 100.9 %all-gather.7.cloned.1.call-done = bf16[2048,1536]{1,0:T(8,128)(2,1)} async-done(((bf16[256,1536]{1,0:T(8,128)(2,1)}), bf16[2048,1536]{1,0:T(8,128)(2,1)}) %all-gather.7.cloned.1.call-update) | async-done | bytes 6291472 | tf_op jit(solution)/shard_map/all_gather | solution.py:26
  135.1 8.5 %fusion.12 = f32[512,1536]{1,0:T(8,128)} fusion(bf16[512,2048]{1,0:T(8,128)(2,1)} %all-gather.5.cloned.1.call-done, bf16[2048,1536]{1,0:T(8,128)(2,1)} %all-gather.7.cloned.1.call-done), kind=kOutput, calls=%fused_computation.25 | convolution fusion | flops 3222798336 | bytes 11534336 | tf_op jit(solution)/shard_map/dot_general | solution.py:24
  143.6 90.6 %all-gather.9.cloned.1.call-done = bf16[2048,1536]{1,0:T(8,128)(2,1)} async-done(((bf16[256,1536]{1,0:T(8,128)(2,1)}), bf16[2048,1536]{1,0:T(8,128)(2,1)}) %all-gather.9.cloned.1.call-update) | async-done | bytes 6291472 | tf_op jit(solution)/shard_map/all_gather | solution.py:27
  234.2 0.0 copy-done.2
  234.2 7.9 %fusion.11 = f32[512,1536]{1,0:T(8,128)} fusion(bf16[512,2048]{1,0:T(8,128)(2,1)S(1)} %copy-done.2, bf16[2048,1536]{1,0:T(8,128)(2,1)} %all-gather.9.cloned.1.call-done), kind=kOutput, calls=%fused_computation.23 | convolution fusion | flops 3222798336 | bytes 11534336 | tf_op jit(solution)/shard_map/dot_general | solution.py:24
  242.1 91.7 %all-gather.11.cloned.1.call-done = bf16[1536,2048]{1,0:T(8,128)(2,1)} async-done(((bf16[1536,256]{1,0:T(8,128)(2,1)}), bf16[1536,2048]{1,0:T(8,128)(2,1)}) %all-gather.11.cloned.1.call-update) | async-done | bytes 6291472 | tf_op jit(solution)/shard_map/all_gather | solution.py:33
  333.8 20.2 %convolution_convert_fusion = bf16[512,2048]{1,0:T(8,128)(2,1)} fusion(bf16[1536,2048]{1,0:T(8,128)(2,1)} %all-gather.11.cloned.1.call-done, f32[512,1536]{1,0:T(8,128)} %fusion.11, f32[512,1536]{1,0:T(8,128)} %fusion.12, f32[1536]{0:T(1024)S(1)} %get-tuple-element.9, f32[1536]{0:T(1024)S(1)} %get-tuple-element.10, f32[1536]{0:T(1024)S(1)} %get-tuple-element.8, ...), kind=kOutput, calls=%fused_computation.21 | convolution fusion | flops 3282042880 | bytes 14716928 | tf_op jit(solution)/shard_map/dot_general | solution.py:31
  354.0 0.0 copy-start
  354.0 0.0 copy-start.1
  354.0 0.0 reduce-scatter.2.cloned.1.call-update
  354.1 29.5 %reduce-scatter.2.cloned.1.call-done = bf16[128,2048]{1,0:T(8,128)(2,1)} async-done(((bf16[512,2048]{1,0:T(8,128)(2,1)}), bf16[128,2048]{1,0:T(8,128)(2,1)}) %reduce-scatter.2.cloned.1.call-update) | async-done | bytes 524304 | tf_op jit(solution)/shard_map/reduce_scatter | solution.py:36
  383.6 1.2 convert_reduce_fusion
  384.8 1.3 fusion.16
  386.1 0.0 copy-done
  386.1 0.0 copy-done.1
  386.1 2.2 fusion.19
  (2 shorter events, 0.0 us)
Async XLA Ops:
  6.5 27.7 %all-gather.5.cloned.1.call-start = ((), (), s32[]{:S(2)}) async-start(), calls=%async_computation.1 | async-start | bytes 2621440 | tf_op jit(solution)/shard_map/all_gather | solution.py:21
  7.3 127.9 %all-gather.7.cloned.1.call-start = ((), (), s32[]{:S(2)}) async-start(), calls=%async_computation.2 | async-start | bytes 7077888 | tf_op jit(solution)/shard_map/all_gather | solution.py:26
  8.0 226.2 %all-gather.9.cloned.1.call-start = ((), (), s32[]{:S(2)}) async-start(), calls=%async_computation.3 | async-start | bytes 7077888 | tf_op jit(solution)/shard_map/all_gather | solution.py:27
  8.7 325.1 %all-gather.11.cloned.1.call-start = ((), (), s32[]{:S(2)}) async-start(), calls=%async_computation.4 | async-start | bytes 7077888 | tf_op jit(solution)/shard_map/all_gather | solution.py:33
  9.3 374.3 %reduce-scatter.2.cloned.1.call-start = ((), (), s32[]{:S(2)}) async-start(), calls=%async_computation.5 | async-start | bytes 2621440 | tf_op jit(solution)/shard_map/reduce_scatter | solution.py:36
  34.2 200.0 %copy-start.2 = (bf16[512,2048]{1,0:T(8,128)(2,1)S(1)}, bf16[512,2048]{1,0:T(8,128)(2,1)}, u32[]{:S(2)}) copy-start(bf16[512,2048]{1,0:T(8,128)(2,1)} %all-gather.5.cloned.1.call-done) | copy-start | bytes 6291460
  354.0 32.1 %copy-start = (f32[2048]{0:T(1024)S(1)}, f32[2048]{0:T(1024)}, u32[]{:S(2)}) copy-start(f32[2048]{0:T(1024)} %param.15) | copy-start | bytes 24580
  354.0 32.1 %copy-start.1 = (f32[2048]{0:T(1024)S(1)}, f32[2048]{0:T(1024)}, u32[]{:S(2)}) copy-start(f32[2048]{0:T(1024)} %param.14) | copy-start | bytes 24580
Sparse Core Ops, SparseCore 0:
  8.9 25.2 all-gather.4
  36.4 98.6 all-gather.6
  137.3 96.8 all-gather.8
  236.1 97.6 all-gather.10
  354.2 29.3 reduce-scatter.1
where the time goes:
time: 395 us
  waiting for transfers between devices  339 us (86%)
  matrix products  36.6 us (9%)
  between operations  13.2 us (3%)
  other arithmetic  4.78 us (1%)
    all_gather x1, waiting for transfers between devices, local(): gate_sum = add_rows(lax.all_gather(gate_weight, 'fs', axis=0, tiled=True))  101 us
    all_gather x1, waiting for transfers between devices, local(): lax.all_gather(down_weight, 'fs', axis=1, tiled=True)  91.7 us
    all_gather x1, waiting for transfers between devices, local(): value_sum = add_rows(lax.all_gather(value_weight, 'fs', axis=0, tiled=True))  90.6 us
    reduce_scatter x1, waiting for transfers between devices, local(): lax.psum_scatter(partial_terms.astype(jnp.bfloat16), 'tp', scatter_dimens...  29.5 us
    all_gather x1, waiting for transfers between devices, local(): sequence = lax.all_gather(tokens, 'tp', axis=0, tiled=True)  23.9 us
    dot_general x1, matrix products, local(): jnp.dot(hidden, lax.all_gather(down_weight, 'fs', axis=1, tiled=True), pr...  20.2 us
    dot_general x2, matrix products, add_rows(): return jnp.dot(sequence, segment, preferred_element_type=jnp.float32)  16.4 us
  transfers between devices with their start and end apart: 5, of which 5 were waited for; matrix products, arithmetic and copies ran while one was open for 4% of the time, Pallas kernels for 0%

commit v1 on v0

--- a/solution.py
+++ b/solution.py
@@ -18,7 +18,12 @@
 def local(
     tokens, gate_weight, value_weight, gate_taps, value_taps, down_weight, norm_gain, norm_shift
 ):
-    sequence = lax.all_gather(tokens, "tp", axis=0, tiled=True)
+    ring = [tokens]
+    for hop in range(3):
+        ring.append(lax.ppermute(ring[-1], "tp", [(dev, (dev + 1) % 4) for dev in range(4)]))
+    sequence = jnp.roll(
+        jnp.concatenate(ring[::-1], axis=0), (lax.axis_index("tp") + 1) * ring[0].shape[0], axis=0
+    )
 
     def add_rows(segment):
         return jnp.dot(sequence, segment, preferred_element_type=jnp.float32)

time: 395 us -> 372 us (0.942)
  waiting for transfers between devices: 339 us -> 307 us
  local copies, waits for them, and re-layouts: 0.99 us -> 7.72 us
    all_gather x1, waiting for transfers between devices: 101 us -> 68.6 us  [local(): gate_sum = add_rows(lax.all_gather(gate_weight, 'fs', axis=0, tiled=True))]
    ppermute x0 -> x3, waiting for transfers between devices: none -> 25.2 us  [local(): lax.ppermute(ring[-1], 'tp', [(dev, (dev + 1) % 4) for dev in range(4)])]
    all_gather x1 -> x0, waiting for transfers between devices: 23.9 us -> none  [local(): sequence = lax.all_gather(tokens, 'tp', axis=0, tiled=True)]
    unnamed x6 -> x13, local copies, waits for them, and re-layouts: 0.01 us -> 5.9 us
  transfers between devices with their start and end apart: 5 -> 7, of which waited for: 5 -> 7; matrix products, arithmetic and copies ran while one was open for 4% -> 7% of each run, Pallas kernels for 0% -> 0%
where the time goes in v1:
time: 372 us; the launch traced here: 371 us
  waiting for transfers between devices  307 us (83%)
  matrix products  37.6 us (10%)
  between operations  13.2 us (4%)
  local copies, waits for them, and re-layouts  7.72 us (2%)
  other arithmetic  4.78 us (1%)
    all_gather x1, waiting for transfers between devices, local(): lax.all_gather(down_weight, 'fs', axis=1, tiled=True)  91.2 us
    all_gather x1, waiting for transfers between devices, local(): value_sum = add_rows(lax.all_gather(value_weight, 'fs', axis=0, tiled=True))  90.6 us
    all_gather x1, waiting for transfers between devices, local(): gate_sum = add_rows(lax.all_gather(gate_weight, 'fs', axis=0, tiled=True))  68.6 us
    reduce_scatter x1, waiting for transfers between devices, local(): lax.psum_scatter(partial_terms.astype(jnp.bfloat16), 'tp', scatter_dimens...  29.5 us
    ppermute x3, waiting for transfers between devices, local(): lax.ppermute(ring[-1], 'tp', [(dev, (dev + 1) % 4) for dev in range(4)])  25.2 us
    dot_general x1, matrix products, local(): jnp.dot(hidden, lax.all_gather(down_weight, 'fs', axis=1, tiled=True), pr...  20.5 us
    dot_general x2, matrix products, add_rows(): return jnp.dot(sequence, segment, preferred_element_type=jnp.float32)  17 us
  transfers between devices with their start and end apart: 7, of which 7 were waited for; matrix products, arithmetic and copies ran while one was open for 7% of the time, Pallas kernels for 0%

profile of v1, /device:TPU:0, one launch (start us, length us, event | category | flops | bytes accessed | tf_op | source)
XLA Modules:
  0.0 371.2 jit_solution(5005801571992568753)
XLA Ops:
  6.5 0.7 all-gather.4.cloned.1.call-update
  7.3 0.0 all-gather.6.cloned.1.call-start
  7.3 0.7 all-gather.6.cloned.1.call-update
  8.0 0.0 all-gather.8.cloned.1.call-start
  8.1 0.7 all-gather.8.cloned.1.call-update
  8.7 0.0 reduce-scatter.2.cloned.1.call-start
  8.8 0.5 collective-permute-start
  9.3 9.0 %collective-permute-done = bf16[128,2048]{1,0:T(8,128)(2,1)S(1)} collective-permute-done((bf16[128,2048]{1,0:T(8,128)(2,1)}, bf16[128,2048]{1,0:T(8,128)(2,1)S(1)}, u32[]{:S(2)}, u32[]{:S(2)}) %collective-permute-start) | collective-permute-done | bytes 524320 | tf_op jit(solution)/shard_map/ppermute | solution.py:23
  18.4 0.0 collective-permute-start.1
  18.4 8.6 %collective-permute-done.1 = bf16[128,2048]{1,0:T(8,128)(2,1)S(1)} collective-permute-done((bf16[128,2048]{1,0:T(8,128)(2,1)S(1)}, bf16[128,2048]{1,0:T(8,128)(2,1)S(1)}, u32[]{:S(2)}, u32[]{:S(2)}) %collective-permute-start.1) | collective-permute-done | bytes 524320 | tf_op jit(solution)/shard_map/ppermute | solution.py:23
  27.0 0.0 collective-permute-start.2
  27.0 1.0 slice_reduce_fusion.2
  27.9 7.6 %collective-permute-done.2 = bf16[128,2048]{1,0:T(8,128)(2,1)S(1)} collective-permute-done((bf16[128,2048]{1,0:T(8,128)(2,1)S(1)}, bf16[128,2048]{1,0:T(8,128)(2,1)S(1)}, u32[]{:S(2)}, u32[]{:S(2)}) %collective-permute-start.2) | collective-permute-done | bytes 524320 | tf_op jit(solution)/shard_map/ppermute | solution.py:23
  35.6 0.8 constant_dynamic-update-slice_fusion.7
  36.4 0.9 constant_dynamic-update-slice_fusion.6
  37.2 0.8 constant_dynamic-update-slice_fusion.5
  38.1 0.9 constant_dynamic-update-slice_fusion.4
  38.9 0.8 constant_dynamic-update-slice_fusion.3
  39.8 0.9 constant_dynamic-update-slice_fusion.2
  40.6 0.8 constant_dynamic-update-slice_fusion.1
  41.5 0.9 constant_dynamic-update-slice_fusion
  42.3 68.6 %all-gather.4.cloned.1.call-done = bf16[2048,1536]{1,0:T(8,128)(2,1)} async-done(((bf16[256,1536]{1,0:T(8,128)(2,1)}), bf16[2048,1536]{1,0:T(8,128)(2,1)}) %all-gather.4.cloned.1.call-update) | async-done | bytes 6291472 | tf_op jit(solution)/shard_map/all_gather | solution.py:31
  111.0 8.5 %fusion.12 = f32[512,1536]{1,0:T(8,128)} fusion(bf16[2048,1536]{1,0:T(8,128)(2,1)} %all-gather.4.cloned.1.call-done, bf16[1024,2048]{1,0:T(8,128)(2,1)} %constant_dynamic-update-slice_fusion, s32[]{:T(128)S(6)} %select_n.14), kind=kOutput, calls=%fused_computation.25 | convolution fusion | flops 3222798336 | bytes 11534340 | tf_op jit(solution)/shard_map/dot_general | solution.py:29
  119.5 90.6 %all-gather.6.cloned.1.call-done = bf16[2048,1536]{1,0:T(8,128)(2,1)} async-done(((bf16[256,1536]{1,0:T(8,128)(2,1)}), bf16[2048,1536]{1,0:T(8,128)(2,1)}) %all-gather.6.cloned.1.call-update) | async-done | bytes 6291472 | tf_op jit(solution)/shard_map/all_gather | solution.py:32
  210.1 8.5 %fusion.11 = f32[512,1536]{1,0:T(8,128)} fusion(bf16[2048,1536]{1,0:T(8,128)(2,1)} %all-gather.6.cloned.1.call-done, bf16[1024,2048]{1,0:T(8,128)(2,1)} %constant_dynamic-update-slice_fusion, s32[]{:T(128)S(6)} %select_n.14), kind=kOutput, calls=%fused_computation.23 | convolution fusion | flops 3222798336 | bytes 11534340 | tf_op jit(solution)/shard_map/dot_general | solution.py:29
  218.6 91.2 %all-gather.8.cloned.1.call-done = bf16[1536,2048]{1,0:T(8,128)(2,1)} async-done(((bf16[1536,256]{1,0:T(8,128)(2,1)}), bf16[1536,2048]{1,0:T(8,128)(2,1)}) %all-gather.8.cloned.1.call-update) | async-done | bytes 6291472 | tf_op jit(solution)/shard_map/all_gather | solution.py:38
  309.8 20.5 %convolution_convert_fusion = bf16[512,2048]{1,0:T(8,128)(2,1)} fusion(bf16[1536,2048]{1,0:T(8,128)(2,1)} %all-gather.8.cloned.1.call-done, f32[512,1536]{1,0:T(8,128)} %fusion.11, f32[512,1536]{1,0:T(8,128)} %fusion.12, f32[1536]{0:T(1024)S(1)} %get-tuple-element.9, f32[1536]{0:T(1024)S(1)} %get-tuple-element.10, f32[1536]{0:T(1024)S(1)} %get-tuple-element.8, ...), kind=kOutput, calls=%fused_computation.21 | convolution fusion | flops 3282042880 | bytes 14716928 | tf_op jit(solution)/shard_map/dot_general | solution.py:36
  330.4 0.0 reduce-scatter.2.cloned.1.call-update
  330.4 29.5 %reduce-scatter.2.cloned.1.call-done = bf16[128,2048]{1,0:T(8,128)(2,1)} async-done(((bf16[512,2048]{1,0:T(8,128)(2,1)}), bf16[128,2048]{1,0:T(8,128)(2,1)}) %reduce-scatter.2.cloned.1.call-update) | async-done | bytes 524304 | tf_op jit(solution)/shard_map/reduce_scatter | solution.py:41
  359.9 1.2 convert_reduce_fusion
  361.1 1.3 fusion.18
  362.4 2.2 fusion.21
  (9 shorter events, 0.0 us)
Async XLA Ops:
  6.5 31.5 %copy-start = (bf16[128,2048]{1,0:T(8,128)(2,1)S(1)}, bf16[128,2048]{1,0:T(8,128)(2,1)}, u32[]{:S(2)}) copy-start(bf16[128,2048]{1,0:T(8,128)(2,1)} %param.8) | copy-start | bytes 1572868
  6.5 104.4 %all-gather.4.cloned.1.call-start = ((), (), s32[]{:S(2)}) async-start(), calls=%async_computation.1 | async-start | bytes 7077888 | tf_op jit(solution)/shard_map/all_gather | solution.py:31
  7.3 202.8 %all-gather.6.cloned.1.call-start = ((), (), s32[]{:S(2)}) async-start(), calls=%async_computation.2 | async-start | bytes 7077888 | tf_op jit(solution)/shard_map/all_gather | solution.py:32
  8.0 301.8 %all-gather.8.cloned.1.call-start = ((), (), s32[]{:S(2)}) async-start(), calls=%async_computation.3 | async-start | bytes 7077888 | tf_op jit(solution)/shard_map/all_gather | solution.py:38
  8.7 351.1 %reduce-scatter.2.cloned.1.call-start = ((), (), s32[]{:S(2)}) async-start(), calls=%async_computation.4 | async-start | bytes 2621440 | tf_op jit(solution)/shard_map/reduce_scatter | solution.py:41
  8.8 9.6 %collective-permute-start = (bf16[128,2048]{1,0:T(8,128)(2,1)}, bf16[128,2048]{1,0:T(8,128)(2,1)S(1)}, u32[]{:S(2)}, u32[]{:S(2)}) collective-permute-start(bf16[128,2048]{1,0:T(8,128)(2,1)} %param.8), channel_id=1, source_target_pairs={{0,1},{1,2},{2,3},{3,0},{4,5},{5,6},{6,7},{7,4},{8,9},{9,10},{10,1... | collective-permute-start | bytes 1572872 | tf_op jit(solution)/shard_map/ppermute | solution.py:23
  18.4 8.6 %collective-permute-start.1 = (bf16[128,2048]{1,0:T(8,128)(2,1)S(1)}, bf16[128,2048]{1,0:T(8,128)(2,1)S(1)}, u32[]{:S(2)}, u32[]{:S(2)}) collective-permute-start(bf16[128,2048]{1,0:T(8,128)(2,1)S(1)} %collective-permute-done), channel_id=1, source_target_pairs={{0,1},{1,2},{2,3},{3,0},{4,5},{5,6},{6,7},{7,4},{8,9},{9,10},{10,1... | collective-permute-start | bytes 1572872 | tf_op jit(solution)/shard_map/ppermute | solution.py:23
  27.0 8.6 %collective-permute-start.2 = (bf16[128,2048]{1,0:T(8,128)(2,1)S(1)}, bf16[128,2048]{1,0:T(8,128)(2,1)S(1)}, u32[]{:S(2)}, u32[]{:S(2)}) collective-permute-start(bf16[128,2048]{1,0:T(8,128)(2,1)S(1)} %collective-permute-done.1), channel_id=1, source_target_pairs={{0,1},{1,2},{2,3},{3,0},{4,5},{5,6},{6,7},{7,4},{8,9},{9,10},{10,1... | collective-permute-start | bytes 1572872 | tf_op jit(solution)/shard_map/ppermute | solution.py:23
  330.3 32.1 %copy-start.1 = (f32[2048]{0:T(1024)S(1)}, f32[2048]{0:T(1024)}, u32[]{:S(2)}) copy-start(f32[2048]{0:T(1024)} %param.15) | copy-start | bytes 24580
  330.3 32.1 %copy-start.2 = (f32[2048]{0:T(1024)S(1)}, f32[2048]{0:T(1024)}, u32[]{:S(2)}) copy-start(f32[2048]{0:T(1024)} %param.14) | copy-start | bytes 24580
Sparse Core Ops, SparseCore 0:
  9.5 101.4 all-gather.3
  113.1 96.8 all-gather.5
  212.1 97.6 all-gather.7
  330.5 29.3 reduce-scatter.1
